TPU v7x, 32 devices: a whole 2x2x4 slice. The times are simulated.
32 devices in a mesh: sp: 8 (over z, y), tp: 4 (over x, core).
Axes of the slice: x: 2, y: 2, z: 4, core: 2. Of those that a mesh axis runs over, the one named last changes fastest.
Arguments:
- resid: bfloat16 [3072, 2048], P('sp', 'tp'), may hold values from -6 to 6
- mixer_in: bfloat16 [3072, 2048], P('sp', 'tp'), may hold values from -6 to 6
- log_step: float32 [3072, 128], P('sp', 'tp'), may hold values from -5.2 to -0.79
- decay_real: float32 [128, 64], P('tp'), may hold values from 0.00016276042 to 0.8
- frequency: float32 [128, 64], P('tp'), may hold values from 0.5 to 6
- input_matrix: float32 [2, 128, 64, 16], P(None, 'tp'), may hold values from -1 to 1
- output_matrix: float32 [2, 128, 16, 64], P(None, 'tp'), may hold values from -0.5 to 0.5
- skip_gain: float32 [2048], P('tp'), may hold values from -4 to 4
- value_weight: bfloat16 [2048, 2048], P(None, 'tp'), may hold values from -0.125 to 0.125
- gate_weight: bfloat16 [2048, 2048], P(None, 'tp'), may hold values from -0.125 to 0.125
- norm_gain: float32 [2048], replicated, may hold values from 0.1 to 1.9
- up_weight: bfloat16 [2048, 8192], P('sp', 'tp'), may hold values from -0.125 to 0.125
- down_weight: bfloat16 [2048, 8192], P('sp', 'tp'), may hold values from -0.0625 to 0.0625
Outputs:
- result: bfloat16 [3072, 2048], P('sp', 'tp')
All inputs are finite; a program needn't handle non-finite values.
Results may differ from a plain program's by a relative error of at most 0.014.
Values may be sent and summed in bfloat16 or wider, within the bound.
A program may use at most 128 MiB of HBM per device.

v0:
```python
import functools

import jax
import jax.numpy as jnp
import numpy as np
from jax import lax
from jax.experimental import pallas as pl
from jax.experimental.pallas import tpu as pltpu
from jax.sharding import PartitionSpec as P

rms_eps = 1e-06
segments = 8
MESH = pl.DeviceIdType.MESH
f32, bf16 = jnp.float32, jnp.bfloat16


def sine_cosine(x):
    y = x * x
    s = 1.0 + y * (-1 / 6 + y * (1 / 120 + y * (-1 / 5040 + y * (1 / 362880 + y * (-1 / 39916800)))))
    c = 1.0 + y * (
        -0.5
        + y * (1 / 24 + y * (-1 / 720 + y * (1 / 40320 + y * (-1 / 3628800 + y * (1 / 479001600)))))
    )
    return x * s, c


def expm1_small(y):
    return y * (
        1.0
        + y * (1 / 2 + y * (1 / 6 + y * (1 / 24 + y * (1 / 120 + y * (1 / 720 + y * (1 / 5040))))))
    )


def kernel(
    n,
    ntp,
    resid_ref,
    mixer_ref,
    step_ref,
    decay_ref,
    angle_ref,
    w_in_ref,
    w_out_ref,
    skip_ref,
    value_ref,
    gate_ref,
    gain_ref,
    up_ref,
    down_ref,
    perm_ref,
    unperm_ref,
    out_ref,
    whole,
    dre,
    dim,
    fre,
    fim,
    step_wide,
    proj,
    ends,
    carries,
    entry,
    mixer_perm,
    mixed_perm,
    chan,
    upd,
    normed,
    hidden,
    parts,
    landed,
    ring_send,
    ring_recv,
    own_sem,
    carry_send,
    carry_recv,
    chan_send,
    chan_recv,
    upd_send,
    upd_recv,
    part_send,
    part_recv,
):
    sp = lax.axis_index("sp")
    tp = lax.axis_index("tp")
    tokens, width = mixer_ref.shape
    block = up_ref.shape[0]
    pieces = ring_send.shape[3]
    piece = block // (2 * pieces)
    groups, states = decay_ref.shape
    each = width // groups
    bunch = min(128 // each, groups)
    chunks = groups // bunch
    lanes, kin = bunch * states, bunch * each
    length = tokens // segments

    odd = sp % 2
    pos = (1 - odd) * (sp // 2) + odd * (n - 1 - sp // 2)

    def at_pos(p):
        p = (p + 2 * n) % n
        high = p // (n // 2)
        return (1 - high) * 2 * p + high * (2 * (n - 1 - p) + 1)

    ahead, behind = at_pos(pos + 1), at_pos(pos - 1)

    barrier = pltpu.get_barrier_semaphore()
    for i in range(1, n):
        pl.semaphore_signal(barrier, inc=1, device_id=((sp + i) % n, tp), device_id_type=MESH)
    for i in range(1, ntp):
        pl.semaphore_signal(barrier, inc=1, device_id=(sp, (tp + i) % ntp), device_id_type=MESH)
    pl.semaphore_wait(barrier, n - 1 + ntp - 1)

    def rows_of(owner, way, part):
        return pl.ds(pl.multiple_of(owner * block + (way * pieces + part) * piece, piece), piece)

    def ring_copy(which, way, k, part, sending):
        source = (up_ref, down_ref)[which]
        sign = -1 if way == 0 else 1
        to = ahead if way == 0 else behind
        shift = k if sending else k + 1
        owner = at_pos(pos + sign * shift)
        slot = whole.at[which, rows_of(owner, way, part)]
        if k == 0 and sending:
            src = source.at[pl.ds((way * pieces + part) * piece, piece)]
        else:
            src = slot
        return pltpu.make_async_remote_copy(
            src_ref=src,
            dst_ref=slot,
            send_sem=ring_send.at[which, way, k, part],
            recv_sem=ring_recv.at[which, way, k, part],
            device_id=(to, tp),
            device_id_type=MESH,
        )

    def service(index):
        which, k = index // (n - 1), index % (n - 1)
        for part in range(pieces):
            for way in range(2):
                if k > 0:
                    ring_copy(which, way, k - 1, part, False).wait_recv()
                ring_copy(which, way, k, part, True).start()

    def finish(which):
        for part in range(pieces):
            for way in range(2):
                ring_copy(which, way, n - 2, part, False).wait_recv()

    queue = list(range(2 * (n - 1)))

    def serve(count=1):
        for _ in range(count):
            if queue:
                service(queue.pop(0))

    own = []
    for which, source in enumerate((up_ref, down_ref)):
        start = pl.multiple_of(sp * block, block)
        c = pltpu.make_async_copy(source, whole.at[which, pl.ds(start, block)], own_sem.at[which])
        c.start()
        own.append(c)
    serve()

    mixer_perm[...] = jnp.dot(
        perm_ref[...], mixer_ref[...], preferred_element_type=f32
    ).astype(bf16)
    highest = lax.Precision.HIGHEST
    step_size = jnp.dot(
        perm_ref[...].astype(f32),
        jnp.exp(step_ref[...]),
        precision=highest,
        preferred_element_type=f32,
    )

    def iota(shape, axis):
        return lax.broadcasted_iota(jnp.int32, shape, axis)

    def ones_where(mask, dtype=f32):
        return jnp.where(mask, 1.0, 0.0).astype(dtype)

    def belongs(rows, columns, span, first):
        gap = iota((rows, columns), 1) + first - iota((rows, columns), 0) * span
        return ones_where((gap >= 0) & (gap < span))

    def tiled(size, copies):
        shape = (size, size * copies)
        hits = jnp.zeros(shape, f32)
        for i in range(copies):
            hits += ones_where(iota(shape, 1) - iota(shape, 0) == i * size)
        return hits

    over_states = tiled(states, bunch)
    over_each = tiled(each, bunch).astype(bf16)
    agree = jnp.zeros((kin, lanes), f32)
    agree_t = jnp.zeros((lanes, kin), f32)
    for i in range(bunch):
        r, l = iota((kin, lanes), 0) - i * each, iota((kin, lanes), 1) - i * states
        agree += ones_where((r >= 0) & (r < each) & (l >= 0) & (l < states))
        r, l = iota((lanes, kin), 1) - i * each, iota((lanes, kin), 0) - i * states
        agree_t += ones_where((r >= 0) & (r < each) & (l >= 0) & (l < states))

    def wide_rate(table, c):
        spread = jnp.dot(table, over_states, precision=highest, preferred_element_type=f32)
        return jnp.sum(
            spread * belongs(groups, lanes, states, c * lanes), axis=0, keepdims=True
        )

    for c in range(chunks):
        cols = pl.ds(c * lanes, lanes)
        step_wide[...] = jnp.dot(
            step_size,
            belongs(groups, lanes, states, c * lanes),
            precision=highest,
            preferred_element_type=f32,
        )
        for i in range(2):
            matrix = jnp.dot(
                w_in_ref[i, c * lanes : (c + 1) * lanes, :].astype(bf16),
                over_each,
                preferred_element_type=f32,
            )
            proj[:, i * lanes : (i + 1) * lanes] = lax.dot_general(
                mixer_perm[:, c * kin : (c + 1) * kin],
                (matrix * agree_t).astype(bf16),
                (((1,), (1,)), ((), ())),
                preferred_element_type=f32,
            )
        rate_row = wide_rate(decay_ref[...], c)
        angle_row = wide_rate(angle_ref[...], c)
        modulus = rate_row * rate_row + angle_row * angle_row
        shape = (segments, lanes)
        rate = jnp.broadcast_to(rate_row, shape)
        half_angle = jnp.broadcast_to(angle_row * 0.5, shape)
        rate_n = jnp.broadcast_to(rate_row / modulus, shape)
        angle_n = jnp.broadcast_to(angle_row / modulus, shape)

        def one(j, state):
            pr, pi, sr, si = state
            rows = pl.ds(pl.multiple_of(j * segments, segments), segments)
            step = step_wide[rows, :]
            s, co = sine_cosine(half_angle * step)
            em = expm1_small(-rate * step)
            factor = 1.0 + em
            twice = 2.0 * s * s
            cos_r = 1.0 - twice
            dr = factor * cos_r
            di = factor * (2.0 * s * co)
            mr = em * cos_r - twice
            vr = di * angle_n - mr * rate_n
            vi = -di * rate_n - mr * angle_n
            a = proj[rows, 0:lanes]
            b = proj[rows, lanes : 2 * lanes]
            fr = vr * a - vi * b
            fi = vr * b + vi * a
            dre[rows, cols] = dr
            dim[rows, cols] = di
            fre[rows, cols] = fr
            fim[rows, cols] = fi
            return (
                dr * pr - di * pi,
                dr * pi + di * pr,
                dr * sr - di * si + fr,
                dr * si + di * sr + fi,
            )

        zero = jnp.zeros(shape, f32)
        last = lax.fori_loop(0, length, one, (zero + 1.0, zero, zero, zero), unroll=2)
        for i in range(4):
            ends[i, :, cols] = last[i]
        serve()

    def link(earlier, later):
        return (
            later[0] * earlier[0] - later[1] * earlier[1] + later[2],
            later[0] * earlier[1] + later[1] * earlier[0] + later[3],
        )

    pr, pi, sr, si = (ends[i, 0:1, :] for i in range(4))
    for s in range(1, segments):
        qr, qi, tr, ti = (ends[i, s : s + 1, :] for i in range(4))
        pr, pi = qr * pr - qi * pi, qr * pi + qi * pr
        sr, si = link((sr, si), (qr, qi, tr, ti))
    for i, v in enumerate((pr, pi, sr, si)):
        carries[sp, i : i + 1, :] = v

    def carry_copy(i, sending):
        there = (sp + i) % n
        slot = sp if sending else (sp + n - i) % n
        return pltpu.make_async_remote_copy(
            src_ref=carries.at[slot],
            dst_ref=carries.at[slot],
            send_sem=carry_send.at[i - 1],
            recv_sem=carry_recv.at[i - 1],
            device_id=(there, tp),
            device_id_type=MESH,
        )

    for i in range(1, n):
        carry_copy(i, True).start()
    for i in range(1, n):
        carry_copy(i, False).wait_recv()
    cr = jnp.zeros_like(pr)
    ci = jnp.zeros_like(pr)
    for d in range(n - 1):
        nr, ni = link((cr, ci), tuple(carries[d, i : i + 1, :] for i in range(4)))
        cr = jnp.where(d < sp, nr, cr)
        ci = jnp.where(d < sp, ni, ci)
    for s in range(segments):
        entry[0, s : s + 1, :] = cr
        entry[1, s : s + 1, :] = ci
        cr, ci = link((cr, ci), tuple(ends[i, s : s + 1, :] for i in range(4)))
    serve()

    for c in range(chunks):
        cols = pl.ds(c * lanes, lanes)

        def again(j, state):
            rows = pl.ds(pl.multiple_of(j * segments, segments), segments)
            dr, di = dre[rows, cols], dim[rows, cols]
            xr, xi = link(state, (dr, di, fre[rows, cols], fim[rows, cols]))
            proj[rows, 0:lanes] = xr
            proj[rows, lanes : 2 * lanes] = xi
            return xr, xi

        lax.fori_loop(0, length, again, (entry[0, :, cols], entry[1, :, cols]), unroll=4)
        ins = slice(c * kin, (c + 1) * kin)
        mech = jnp.zeros((tokens, kin), f32)
        for i in range(2):
            matrix = jnp.dot(
                w_out_ref[i, c * kin : (c + 1) * kin, :].astype(bf16),
                over_states.astype(bf16),
                preferred_element_type=f32,
            )
            mech += (1 - 2 * i) * lax.dot_general(
                proj[:, i * lanes : (i + 1) * lanes].astype(bf16),
                (matrix * agree).astype(bf16),
                (((1,), (1,)), ((), ())),
                preferred_element_type=f32,
            )
        mech = mech + skip_ref[0:1, ins] * mixer_perm[:, ins].astype(f32)
        mixed_perm[:, ins] = jax.nn.gelu(mech).astype(bf16)
        if c % 2 == 1:
            serve()
    chan[tp] = jnp.dot(unperm_ref[...], mixed_perm[...], preferred_element_type=f32).astype(bf16)

    def tp_copy(buf, sems, i, sending):
        slot = tp if sending else (tp + ntp - i) % ntp
        return pltpu.make_async_remote_copy(
            src_ref=buf.at[slot],
            dst_ref=buf.at[slot],
            send_sem=sems[0].at[i - 1],
            recv_sem=sems[1].at[i - 1],
            device_id=(sp, (tp + i) % ntp),
            device_id_type=MESH,
        )

    chan_sems, upd_sems = (chan_send, chan_recv), (upd_send, upd_recv)
    for i in range(1, ntp):
        tp_copy(chan, chan_sems, i, True).start()
    serve()
    for i in range(1, ntp):
        tp_copy(chan, chan_sems, i, False).wait_recv()

    tile = 256

    @pl.loop(0, width // tile)
    def _(t):
        cols = pl.ds(pl.multiple_of(t * tile, tile), tile)
        v = jnp.zeros((tokens, tile), f32)
        g = jnp.zeros((tokens, tile), f32)
        for q in range(ntp):
            rows = slice(q * width, (q + 1) * width)
            v += jnp.dot(chan[q], value_ref[rows, cols], preferred_element_type=f32)
            g += jnp.dot(chan[q], gate_ref[rows, cols], preferred_element_type=f32)
        upd[tp, :, cols] = (resid_ref[:, cols].astype(f32) + v * jax.nn.sigmoid(g)).astype(bf16)

    for i in range(1, ntp):
        tp_copy(upd, upd_sems, i, True).start()
    serve()
    for i in range(1, ntp):
        tp_copy(upd, upd_sems, i, False).wait_recv()

    total = jnp.zeros((tokens, 1), f32)
    for q in range(ntp):
        u = upd[q].astype(f32)
        total += jnp.sum(u * u, axis=1, keepdims=True)
    inv = lax.rsqrt(total * (1.0 / (width * ntp)) + rms_eps)
    for q in range(ntp):
        cols = slice(q * width, (q + 1) * width)
        normed[:, cols] = (upd[q].astype(f32) * inv * gain_ref[0:1, cols]).astype(bf16)

    while queue and queue[0] < n - 1:
        serve()
    for c in own:
        c.wait()
    if queue and queue[0] == n - 1:
        serve()
    finish(0)

    @pl.loop(0, hidden.shape[1] // tile)
    def _(t):
        cols = pl.ds(pl.multiple_of(t * tile, tile), tile)
        r = jnp.dot(normed[...], whole[0, :, cols], preferred_element_type=f32)
        r = jnp.maximum(r, 0.0)
        hidden[:, cols] = (r * r).astype(bf16)

    per = 2 * n // ntp
    half = block // 2

    def part_copy(h):
        return pltpu.make_async_remote_copy(
            src_ref=parts.at[h],
            dst_ref=landed.at[tp, h % per],
            send_sem=part_send.at[h],
            recv_sem=part_recv.at[tp, h % per],
            device_id=(sp, h // per),
            device_id_type=MESH,
        )

    def down_part(owner, way):
        h = 2 * owner + way
        rows = pl.ds(pl.multiple_of(h * half, half), half)
        p = lax.dot_general(
            hidden[...],
            whole[1, rows, :],
            (((1,), (1,)), ((), ())),
            preferred_element_type=f32,
        )
        parts[h] = p.astype(bf16)

        @pl.when(h // per != tp)
        def _():
            part_copy(h).start()

    down_part(sp, 0)
    down_part(sp, 1)
    for k in range(n - 1):
        if k < n - 2:
            while queue and queue[0] <= n + k:
                serve()
        else:
            finish(1)
        down_part(at_pos(pos - k - 1), 0)
        down_part(at_pos(pos + k + 1), 1)

    for i in range(1, ntp):
        there = (tp + i) % ntp
        for t in range(per):
            pltpu.make_async_remote_copy(
                src_ref=parts.at[t],
                dst_ref=landed.at[there, t],
                send_sem=part_send.at[t],
                recv_sem=part_recv.at[there, t],
                device_id=(sp, there),
                device_id_type=MESH,
            ).wait_recv()
    for t in range(per):
        cols = slice(t * half, (t + 1) * half)
        acc = parts[tp * per + t].astype(f32)
        for i in range(1, ntp):
            acc += landed[(tp + i) % ntp, t].astype(f32)
        out_ref[:, cols] = (upd[tp, :, cols].astype(f32) + acc).astype(bf16)

    for which in range(2):
        for k in range(n - 1):
            for way in range(2):
                for part in range(pieces):
                    ring_copy(which, way, k, part, True).wait_send()
    for i in range(1, n):
        carry_copy(i, True).wait_send()
    for i in range(1, ntp):
        tp_copy(chan, chan_sems, i, True).wait_send()
        tp_copy(upd, upd_sems, i, True).wait_send()
    for h in range(2 * n):

        @pl.when(h // per != tp)
        def _():
            part_copy(h).wait_send()


def per_device(
    n,
    ntp,
    resid,
    mixer_in,
    log_step,
    decay_real,
    frequency,
    input_matrix,
    output_matrix,
    skip_gain,
    value_weight,
    gate_weight,
    norm_gain,
    up_weight,
    down_weight,
):
    tokens, width = mixer_in.shape
    groups, states = decay_real.shape
    per = width // groups
    bunch = min(128 // per, groups)
    chunks = groups // bunch
    kin, lanes = bunch * per, bunch * states
    features, units = value_weight.shape[0], up_weight.shape[1]
    length = tokens // segments
    row = np.arange(tokens)
    perm = (row[None, :] == ((row % segments) * length + row // segments)[:, None]).astype(np.float32)
    pieces = 2
    total = groups * states
    dma = pltpu.SemaphoreType.DMA
    vmem = pl.BlockSpec(memory_space=pltpu.VMEM)
    return pl.pallas_call(
        functools.partial(kernel, n, ntp),
        out_shape=jax.ShapeDtypeStruct((tokens, width), bf16),
        in_specs=[vmem] * 15,
        out_specs=vmem,
        scratch_shapes=[
            pltpu.VMEM((2, features, units), bf16),
            pltpu.VMEM((tokens, total), f32),
            pltpu.VMEM((tokens, total), f32),
            pltpu.VMEM((tokens, total), f32),
            pltpu.VMEM((tokens, total), f32),
            pltpu.VMEM((tokens, lanes), f32),
            pltpu.VMEM((tokens, 2 * lanes), f32),
            pltpu.VMEM((4, segments, total), f32),
            pltpu.VMEM((n, 4, total), f32),
            pltpu.VMEM((2, segments, total), f32),
            pltpu.VMEM((tokens, width), bf16),
            pltpu.VMEM((tokens, width), bf16),
            pltpu.VMEM((ntp, tokens, width), bf16),
            pltpu.VMEM((ntp, tokens, width), bf16),
            pltpu.VMEM((tokens, features), bf16),
            pltpu.VMEM((tokens, units), bf16),
            pltpu.VMEM((2 * n, tokens, features // (2 * n)), bf16),
            pltpu.VMEM((ntp, 2 * n // ntp, tokens, features // (2 * n)), bf16),
            dma((2, 2, n - 1, pieces)),
            dma((2, 2, n - 1, pieces)),
            dma((2,)),
            dma((n - 1,)),
            dma((n - 1,)),
            dma((ntp - 1,)),
            dma((ntp - 1,)),
            dma((ntp - 1,)),
            dma((ntp - 1,)),
            dma((2 * n,)),
            dma((ntp, 2 * n // ntp)),
        ],
        compiler_params=pltpu.CompilerParams(
            collective_id=0, has_side_effects=True, vmem_limit_bytes=64 * 1024 * 1024 - 65536
        ),
    )(
        resid,
        mixer_in,
        log_step,
        decay_real,
        frequency,
        input_matrix.reshape(2, groups * states, per),
        output_matrix.reshape(2, groups * per, states),
        skip_gain.reshape(1, width),
        value_weight,
        gate_weight,
        norm_gain.reshape(1, features),
        up_weight,
        down_weight,
        jnp.asarray(perm, bf16),
        jnp.asarray(perm.T, bf16),
    )


def solution(mesh):
    in_specs = (
        P("sp", "tp"),
        P("sp", "tp"),
        P("sp", "tp"),
        P("tp", None),
        P("tp", None),
        P(None, "tp", None, None),
        P(None, "tp", None, None),
        P("tp"),
        P(None, "tp"),
        P(None, "tp"),
        P(),
        P("sp", "tp"),
        P("sp", "tp"),
    )
    body = functools.partial(per_device, mesh.shape["sp"], mesh.shape["tp"])
    return jax.shard_map(
        body, mesh=mesh, in_specs=in_specs, out_specs=P("sp", "tp"), check_vma=False
    )
```

profile of v0, /device:TPU:0, one launch (start us, length us, event | category | flops | bytes accessed | tf_op | source)
XLA Modules:
  0.0 194.8 jit_solution(1021809575680240563)
XLA Ops:
  0.0 1.6 copy.17.step_ref
  1.6 3.0 %copy.16 = f32[2,32,64,16]{3,2,1,0:T(8,128)} copy(f32[2,32,64,16]{2,3,1,0:T(8,128)} %param.20) | data formatting | bytes 524288 | tf_op args[5]
  4.6 188.4 %shard_map.145 = bf16[384,512]{1,0:T(8,128)(2,1)} custom-call(bf16[384,512]{1,0:T(8,128)(2,1)} %resid_ref.1, bf16[384,512]{1,0:T(8,128)(2,1)} %mixer_ref.1, f32[384,32]{1,0:T(8,128)} %copy.17.step_ref, f32[32,64]{1,0:T(8,128)} %decay_ref.1, f32[32,64]{1,0:T(8,128)} %angle_ref.1, f32[2,2048,16]{2,1,0:T(8,128)} %bitcast.4, f32[2,512,64]{2,1,0:T(8,128)} %bitcast.5, ...), custom_call_target="tpu_custom_call" | custom-call | tf_op jit(solution)/shard_map/pallas_call | solution.py:512
  193.0 1.8 copy.19
where the time goes:
time: 195 us
  Pallas kernels  188 us (96%)
  local copies, waits for them, and re-layouts  6.39 us (3%)
    pallas_call x1, Pallas kernels, per_device(): pl.pallas_call(functools.partial(kernel, n, ntp), out_shape=jax.ShapeDtyp...  188 us
    unnamed x3, local copies, waits for them, and re-layouts  6.39 us

commit v1 on v0

v1 whole, which is shorter than its diff:
```python
import functools

import jax
import jax.numpy as jnp
import numpy as np
from jax import lax
from jax.experimental import pallas as pl
from jax.experimental.pallas import tpu as pltpu
from jax.sharding import PartitionSpec as P

rms_eps = 1e-06
segments = 8
MESH = pl.DeviceIdType.MESH
f32, bf16 = jnp.float32, jnp.bfloat16


def sine_cosine(x):
    y = x * x
    s = 1.0 + y * (-1 / 6 + y * (1 / 120 + y * (-1 / 5040 + y * (1 / 362880 + y * (-1 / 39916800)))))
    c = 1.0 + y * (
        -0.5
        + y * (1 / 24 + y * (-1 / 720 + y * (1 / 40320 + y * (-1 / 3628800 + y * (1 / 479001600)))))
    )
    return x * s, c


def expm1_small(y):
    return y * (
        1.0
        + y * (1 / 2 + y * (1 / 6 + y * (1 / 24 + y * (1 / 120 + y * (1 / 720 + y * (1 / 5040))))))
    )


def kernel(
    n,
    ntp,
    resid_ref,
    mixer_ref,
    step_ref,
    decay_ref,
    angle_ref,
    w_in_ref,
    w_out_ref,
    skip_ref,
    value_hbm,
    gate_hbm,
    gain_ref,
    up_hbm,
    down_hbm,
    perm_ref,
    unperm_ref,
    out_ref,
    up_whole,
    down_whole,
    value_ref,
    gate_ref,
    dre,
    dim,
    fre,
    fim,
    step_wide,
    proj,
    ends,
    carries,
    entry,
    mixer_perm,
    chan,
    upd,
    normed,
    hidden,
    keep,
    out1,
    in1,
    out2,
    in2,
    out3,
    in3,
    own_sem,
    z_send,
    z_recv,
    y_send,
    y_recv,
    carry_send,
    carry_recv,
    chan_core_send,
    chan_core_recv,
    chan_x_send,
    chan_x_recv,
    upd_z_send,
    upd_z_recv,
    upd_core_send,
    upd_core_recv,
    upd_x_send,
    upd_x_recv,
    sum1_send,
    sum1_recv,
    sum2_send,
    sum2_recv,
    sum3_send,
    sum3_recv,
):
    sp = lax.axis_index("sp")
    tp = lax.axis_index("tp")
    tokens, width = mixer_ref.shape
    block = up_hbm.shape[0]
    units = up_whole.shape[1]
    groups, states = decay_ref.shape
    each = width // groups
    bunch = min(128 // each, groups)
    chunks = groups // bunch
    lanes, kin = bunch * states, bunch * each
    length = tokens // segments
    pieces = z_send.shape[2]
    piece = block // pieces
    nz, nx, per = n // 2, ntp // 2, n // ntp
    z, y = sp // 2, sp % 2
    x, core = tp // 2, tp % 2
    partner = tp + 1 - 2 * core

    def xor(a, k):
        total = 0
        bit = 1
        while bit < nz:
            digit = (a // bit) % 2
            total = total + bit * (1 - digit if k & bit else digit)
            bit *= 2
        return total

    def flip(a):
        return a + 1 - 2 * (a % 2)

    pair_z = flip(z)
    pair = 2 * pair_z + y
    inner = ((z + 1) // 2) % 2

    barrier = pltpu.get_barrier_semaphore()
    for i in range(1, n):
        pl.semaphore_signal(barrier, inc=1, device_id=((sp + i) % n, tp), device_id_type=MESH)
    for i in range(1, ntp):
        pl.semaphore_signal(barrier, inc=1, device_id=(sp, (tp + i) % ntp), device_id_type=MESH)
    pl.semaphore_wait(barrier, n - 1 + ntp - 1)

    sources, wholes = (up_hbm, down_hbm), (up_whole, down_whole)

    def rows_of(owner, part=None):
        if part is None:
            return pl.ds(pl.multiple_of(owner * block, block), block)
        return pl.ds(pl.multiple_of(owner * block + part * piece, piece), piece)

    def columns_for(a):
        return pl.ds(pl.multiple_of((a % 2) * units, units), units)

    def z_copy(which, k, zk, part, sending):
        owner = sp if sending else 2 * zk + y
        return pltpu.make_async_remote_copy(
            src_ref=sources[which].at[pl.ds(part * piece, piece), columns_for(zk)],
            dst_ref=wholes[which].at[rows_of(owner, part)],
            send_sem=z_send.at[which, k, part],
            recv_sem=z_recv.at[which, k, part],
            device_id=(2 * zk + y, tp),
            device_id_type=MESH,
        )

    def y_copy(which, k, zk, part, sending):
        owner = 2 * zk + (y if sending else 1 - y)
        slot = wholes[which].at[rows_of(owner, part)]
        src = slot
        if isinstance(k, int) and k == 0:
            src = sources[which].at[pl.ds(part * piece, piece), columns_for(z)]
        return pltpu.make_async_remote_copy(
            src_ref=src,
            dst_ref=slot,
            send_sem=y_send.at[which, k, part],
            recv_sem=y_recv.at[which, k, part],
            device_id=(2 * z + 1 - y, tp),
            device_id_type=MESH,
        )

    def z_start(which, k):
        for part in range(pieces):
            z_copy(which, k, xor(z, k), part, True).start()

    def forward(which, k, zk):
        for part in range(pieces):
            z_copy(which, k, zk, part, False).wait_recv()
            y_copy(which, k, zk, part, True).start()

    def y_arrived(which, k, zk):
        for part in range(pieces):
            y_copy(which, k, zk, part, False).wait_recv()

    far = []
    for base in range(2, nz, 2):
        zb = xor(z, base)
        zf = flip(zb)
        far.append((base + inner, zb + inner * (zf - zb)))
        far.append((base + 1 - inner, zf + inner * (zb - zf)))
    near, distant = far[0::2], far[1::2]

    own = []
    for which in range(2):
        c = pltpu.make_async_copy(
            sources[which].at[:, columns_for(z)], wholes[which].at[rows_of(sp)], own_sem.at[which]
        )
        c.start()
        own.append(c)
    for which in range(2):
        for part in range(pieces):
            y_copy(which, 0, z, part, True).start()
        z_start(which, 1)
    for k in range(2, nz):
        z_start(0, k)
    gates = []
    for which, (source, target) in enumerate(((value_hbm, value_ref), (gate_hbm, gate_ref))):
        c = pltpu.make_async_copy(source, target, own_sem.at[2 + which])
        c.start()
        gates.append(c)

    def far_down():
        for k in range(2, nz):
            z_start(1, k)

    def tp_at(a, b):
        return 2 * a + b

    def chan_core(i, c, sending):
        cols = pl.ds(c * kin, kin)
        slot = tp_at((x + nx - i) % nx, core if sending else 1 - core)
        return pltpu.make_async_remote_copy(
            src_ref=chan.at[slot, :, cols],
            dst_ref=chan.at[slot, :, cols],
            send_sem=chan_core_send.at[i, c],
            recv_sem=chan_core_recv.at[i, c],
            device_id=(sp, partner),
            device_id_type=MESH,
        )

    def chan_x(i, c, sending):
        cols = pl.ds(c * kin, kin)
        slot = tp if sending else tp_at((x + nx - i) % nx, core)
        return pltpu.make_async_remote_copy(
            src_ref=chan.at[slot, :, cols],
            dst_ref=chan.at[slot, :, cols],
            send_sem=chan_x_send.at[i - 1, c],
            recv_sem=chan_x_recv.at[i - 1, c],
            device_id=(sp, tp_at((x + i) % nx, core)),
            device_id_type=MESH,
        )

    def chan_forward(c):
        for i in range(1, nx):
            chan_x(i, c, False).wait_recv()
            chan_core(i, c, True).start()

    mixer_perm[...] = jnp.dot(
        perm_ref[...], mixer_ref[...], preferred_element_type=f32
    ).astype(bf16)
    highest = lax.Precision.HIGHEST
    step_size = lax.dot_general(
        perm_ref[...].astype(f32),
        jnp.exp(step_ref[...]),
        (((1,), (1,)), ((), ())),
        precision=highest,
        preferred_element_type=f32,
    )

    def iota(shape, axis):
        return lax.broadcasted_iota(jnp.int32, shape, axis)

    def ones_where(mask, dtype=f32):
        return jnp.where(mask, 1.0, 0.0).astype(dtype)

    def belongs(rows, columns, span, first):
        gap = iota((rows, columns), 1) + first - iota((rows, columns), 0) * span
        return ones_where((gap >= 0) & (gap < span))

    def tiled(size, copies):
        shape = (size, size * copies)
        hits = jnp.zeros(shape, f32)
        for i in range(copies):
            hits += ones_where(iota(shape, 1) - iota(shape, 0) == i * size)
        return hits

    over_states = tiled(states, bunch)
    agree = jnp.zeros((kin, lanes), f32)
    for i in range(bunch):
        r, l = iota((kin, lanes), 0) - i * each, iota((kin, lanes), 1) - i * states
        agree += ones_where((r >= 0) & (r < each) & (l >= 0) & (l < states))

    def wide_rate(table, c):
        spread = jnp.dot(table, over_states, precision=highest, preferred_element_type=f32)
        return jnp.sum(
            spread * belongs(groups, lanes, states, c * lanes), axis=0, keepdims=True
        )

    for c in range(chunks):
        cols = pl.ds(c * lanes, lanes)
        step_wide[...] = jnp.dot(
            step_size,
            belongs(groups, lanes, states, c * lanes),
            precision=highest,
            preferred_element_type=f32,
        )
        for i in range(2):
            matrix = jnp.dot(
                w_in_ref[i, c * kin : (c + 1) * kin, :].astype(bf16),
                over_states.astype(bf16),
                preferred_element_type=f32,
            )
            proj[:, i * lanes : (i + 1) * lanes] = jnp.dot(
                mixer_perm[:, c * kin : (c + 1) * kin],
                (matrix * agree).astype(bf16),
                preferred_element_type=f32,
            )
        rate_row = wide_rate(decay_ref[...], c)
        angle_row = wide_rate(angle_ref[...], c)
        modulus = rate_row * rate_row + angle_row * angle_row
        shape = (segments, lanes)
        rate = jnp.broadcast_to(rate_row, shape)
        half_angle = jnp.broadcast_to(angle_row * 0.5, shape)
        rate_n = jnp.broadcast_to(rate_row / modulus, shape)
        angle_n = jnp.broadcast_to(angle_row / modulus, shape)

        def one(j, state):
            pr, pi, sr, si = state
            rows = pl.ds(pl.multiple_of(j * segments, segments), segments)
            step = step_wide[rows, :]
            s, co = sine_cosine(half_angle * step)
            em = expm1_small(-rate * step)
            factor = 1.0 + em
            twice = 2.0 * s * s
            cos_r = 1.0 - twice
            dr = factor * cos_r
            di = factor * (2.0 * s * co)
            mr = em * cos_r - twice
            vr = di * angle_n - mr * rate_n
            vi = -di * rate_n - mr * angle_n
            a = proj[rows, 0:lanes]
            b = proj[rows, lanes : 2 * lanes]
            fr = vr * a - vi * b
            fi = vr * b + vi * a
            dre[rows, cols] = dr
            dim[rows, cols] = di
            fre[rows, cols] = fr
            fim[rows, cols] = fi
            return (
                dr * pr - di * pi,
                dr * pi + di * pr,
                dr * sr - di * si + fr,
                dr * si + di * sr + fi,
            )

        zero = jnp.zeros(shape, f32)
        last = lax.fori_loop(0, length, one, (zero + 1.0, zero, zero, zero), unroll=2)
        for i in range(4):
            ends[i, :, cols] = last[i]
        if c >= chunks - 2:
            forward(c - chunks + 2, 1, pair_z)

    def link(earlier, later):
        return (
            later[0] * earlier[0] - later[1] * earlier[1] + later[2],
            later[0] * earlier[1] + later[1] * earlier[0] + later[3],
        )

    pr, pi, sr, si = (ends[i, 0:1, :] for i in range(4))
    for s in range(1, segments):
        qr, qi, tr, ti = (ends[i, s : s + 1, :] for i in range(4))
        pr, pi = qr * pr - qi * pi, qr * pi + qi * pr
        sr, si = link((sr, si), (qr, qi, tr, ti))
    for i, v in enumerate((pr, pi, sr, si)):
        carries[sp, i : i + 1, :] = v

    def carry_copy(i, sending):
        there = (sp + i) % n
        slot = sp if sending else (sp + n - i) % n
        return pltpu.make_async_remote_copy(
            src_ref=carries.at[slot],
            dst_ref=carries.at[slot],
            send_sem=carry_send.at[i - 1],
            recv_sem=carry_recv.at[i - 1],
            device_id=(there, tp),
            device_id_type=MESH,
        )

    for i in range(1, n):
        carry_copy(i, True).start()
    for i in range(1, n):
        carry_copy(i, False).wait_recv()
    cr = jnp.zeros_like(pr)
    ci = jnp.zeros_like(pr)
    for d in range(n - 1):
        nr, ni = link((cr, ci), tuple(carries[d, i : i + 1, :] for i in range(4)))
        cr = jnp.where(d < sp, nr, cr)
        ci = jnp.where(d < sp, ni, ci)
    for s in range(segments):
        entry[0, s : s + 1, :] = cr
        entry[1, s : s + 1, :] = ci
        cr, ci = link((cr, ci), tuple(ends[i, s : s + 1, :] for i in range(4)))

    for c in range(chunks):
        cols = pl.ds(c * lanes, lanes)

        def again(j, state):
            rows = pl.ds(pl.multiple_of(j * segments, segments), segments)
            dr, di = dre[rows, cols], dim[rows, cols]
            xr, xi = link(state, (dr, di, fre[rows, cols], fim[rows, cols]))
            proj[rows, 0:lanes] = xr
            proj[rows, lanes : 2 * lanes] = xi
            return xr, xi

        lax.fori_loop(0, length, again, (entry[0, :, cols], entry[1, :, cols]), unroll=4)
        ins = slice(c * kin, (c + 1) * kin)
        mech = jnp.zeros((tokens, kin), f32)
        for i in range(2):
            matrix = jnp.dot(
                w_out_ref[i, c * kin : (c + 1) * kin, :].astype(bf16),
                over_states.astype(bf16),
                preferred_element_type=f32,
            )
            mech += (1 - 2 * i) * lax.dot_general(
                proj[:, i * lanes : (i + 1) * lanes].astype(bf16),
                (matrix * agree).astype(bf16),
                (((1,), (1,)), ((), ())),
                preferred_element_type=f32,
            )
        mech = mech + skip_ref[0:1, ins] * mixer_perm[:, ins].astype(f32)
        mixed = jax.nn.gelu(mech).astype(bf16)
        chan[tp, :, ins] = jnp.dot(
            unperm_ref[...], mixed, preferred_element_type=f32
        ).astype(bf16)
        chan_core(0, c, True).start()
        for i in range(1, nx):
            chan_x(i, c, True).start()
        if c >= 2:
            chan_forward(c - 2)

    @pl.when(inner == 1)
    def _():
        far_down()

    for k, zk in near + distant:
        forward(0, k, zk)
    for c in range(max(chunks - 2, 0), chunks):
        chan_forward(c)
    for c in gates:
        c.wait()
    for c in range(chunks):
        for i in range(nx):
            chan_core(i, c, False).wait_recv()

    tile = 256

    @pl.loop(0, width // tile)
    def _(t):
        cols = pl.ds(pl.multiple_of(t * tile, tile), tile)
        v = jnp.zeros((tokens, tile), f32)
        g = jnp.zeros((tokens, tile), f32)
        for q in range(ntp):
            rows = slice(q * width, (q + 1) * width)
            v += jnp.dot(chan[q], value_ref[rows, cols], preferred_element_type=f32)
            g += jnp.dot(chan[q], gate_ref[rows, cols], preferred_element_type=f32)
        upd[0, tp, :, cols] = (resid_ref[:, cols].astype(f32) + v * jax.nn.sigmoid(g)).astype(bf16)

    def upd_z():
        return pltpu.make_async_remote_copy(
            src_ref=upd.at[0, tp],
            dst_ref=upd.at[1, tp],
            send_sem=upd_z_send.at[0],
            recv_sem=upd_z_recv.at[0],
            device_id=(pair, tp),
            device_id_type=MESH,
        )

    def upd_x(i, h, sending):
        slot = tp if sending else tp_at((x + nx - i) % nx, core)
        return pltpu.make_async_remote_copy(
            src_ref=upd.at[h, slot],
            dst_ref=upd.at[h, slot],
            send_sem=upd_x_send.at[i - 1, h],
            recv_sem=upd_x_recv.at[i - 1, h],
            device_id=(sp, tp_at((x + i) % nx, core)),
            device_id_type=MESH,
        )

    def upd_core(i, h, sending):
        slot = tp_at((x + nx - i) % nx, core if sending else 1 - core)
        return pltpu.make_async_remote_copy(
            src_ref=upd.at[h, slot],
            dst_ref=upd.at[h, slot],
            send_sem=upd_core_send.at[i, h],
            recv_sem=upd_core_recv.at[i, h],
            device_id=(sp, partner),
            device_id_type=MESH,
        )

    upd_z().start()
    for i in range(1, nx):
        upd_x(i, 0, True).start()
    upd_core(0, 0, True).start()

    @pl.when(inner == 0)
    def _():
        far_down()

    for i in range(1, nx):
        upd_x(i, 0, False).wait_recv()
        upd_core(i, 0, True).start()
    upd_z().wait_recv()
    for i in range(1, nx):
        upd_x(i, 1, True).start()
    upd_core(0, 1, True).start()

    def normalize(h):
        for i in range(nx):
            upd_core(i, h, False).wait_recv()
        total = jnp.zeros((tokens, 1), f32)
        for q in range(ntp):
            u = upd[h, q].astype(f32)
            total += jnp.sum(u * u, axis=1, keepdims=True)
        inv = lax.rsqrt(total * (1.0 / (width * ntp)) + rms_eps)
        for q in range(ntp):
            cols = slice(q * width, (q + 1) * width)
            normed[:, cols] = (upd[h, q].astype(f32) * inv * gain_ref[0:1, cols]).astype(bf16)

    def raise_up(h):
        @pl.loop(0, units // tile)
        def _(t):
            cols = pl.ds(pl.multiple_of(t * tile, tile), tile)
            r = jnp.dot(normed[...], up_whole[:, cols], preferred_element_type=f32)
            r = jnp.maximum(r, 0.0)
            hidden[h * tokens : (h + 1) * tokens, cols] = (r * r).astype(bf16)

    normalize(0)
    for c in own:
        c.wait()
    y_arrived(0, 0, z)
    y_arrived(0, 1, pair_z)
    for k, zk in far:
        y_arrived(0, k, zk)
    raise_up(0)
    for i in range(1, nx):
        upd_x(i, 1, False).wait_recv()
        upd_core(i, 1, True).start()
    normalize(1)
    raise_up(1)

    def sum1(s):
        return pltpu.make_async_remote_copy(
            src_ref=out1.at[s],
            dst_ref=in1.at[s],
            send_sem=sum1_send.at[s],
            recv_sem=sum1_recv.at[s],
            device_id=(sp, partner),
            device_id_type=MESH,
        )

    def sum2(s):
        return pltpu.make_async_remote_copy(
            src_ref=out2.at[s],
            dst_ref=in2.at[s % per, x],
            send_sem=sum2_send.at[s],
            recv_sem=sum2_recv.at[s % per, x],
            device_id=(sp, s // per),
            device_id_type=MESH,
        )

    def sum3(j):
        return pltpu.make_async_remote_copy(
            src_ref=out3.at[j],
            dst_ref=in3.at[j],
            send_sem=sum3_send.at[j],
            recv_sem=sum3_recv.at[j],
            device_id=(pair, tp),
            device_id_type=MESH,
        )

    def core_of(s):
        return (s // per) % 2

    def x_of(s):
        return s // per // 2

    def stage1(s):
        rows = rows_of(s)

        @pl.loop(0, 2)
        def _(h):
            some = pl.ds(pl.multiple_of(h * tokens, tokens), tokens)
            keep[s, some, :] = lax.dot_general(
                hidden[some, :],
                down_whole[rows, :],
                (((1,), (1,)), ((), ())),
                preferred_element_type=f32,
            )

        @pl.when(core_of(s) != core)
        def _():
            out1[s] = keep[s].astype(bf16)
            sum1(s).start()

    def stage2(s):
        @pl.when(core_of(s) == core)
        def _():
            sum1(s).wait_recv()
            total = keep[s] + in1[s].astype(f32)

            @pl.when(x_of(s) == x)
            def _():
                keep[s] = total

            @pl.when(x_of(s) != x)
            def _():
                out2[s] = total.astype(bf16)
                sum2(s).start()

    def stage3(s):
        j = s % per

        @pl.when(s // per == tp)
        def _():
            total = keep[s]
            for i in range(1, nx):
                there = (x + i) % nx
                pltpu.make_async_remote_copy(
                    src_ref=out2.at[s],
                    dst_ref=in2.at[j, there],
                    send_sem=sum2_send.at[s],
                    recv_sem=sum2_recv.at[j, there],
                    device_id=(sp, tp_at(there, core)),
                    device_id_type=MESH,
                ).wait_recv()
                total += in2[j, there].astype(f32)
            keep[s] = total
            out3[j] = total[tokens:].astype(bf16)
            sum3(j).start()

    order = []

    def step(k, zk, side):
        if side == 1:
            y_arrived(1, k, zk)
        s = 2 * zk + (y if side == 0 else 1 - y)
        stage1(s)
        order.append(s)
        if len(order) > 1:
            stage2(order[-2])
        if len(order) > 3:
            stage3(order[-4])

    for k, zk in near:
        forward(1, k, zk)
    for side in range(2):
        step(0, z, side)
    for side in range(2):
        step(1, pair_z, side)
    for k, zk in near:
        for side in range(2):
            step(k, zk, side)
    for k, zk in distant:
        forward(1, k, zk)
    for k, zk in distant:
        for side in range(2):
            step(k, zk, side)
    stage2(order[-1])
    for s in order[-3:]:
        stage3(s)
    for j in range(per):
        s = tp * per + j
        sum3(j).wait_recv()
        cols = slice(j * block, (j + 1) * block)
        total = keep[s, :tokens] + in3[j].astype(f32)
        out_ref[:, cols] = (upd[0, tp, :, cols].astype(f32) + total).astype(bf16)

    for which in range(2):
        for k in range(nz):
            for part in range(pieces):
                y_copy(which, k, xor(z, k), part, True).wait_send()
                if k > 0:
                    z_copy(which, k, xor(z, k), part, True).wait_send()
    for i in range(1, n):
        carry_copy(i, True).wait_send()
    for i in range(nx):
        for c in range(chunks):
            chan_core(i, c, True).wait_send()
            if i > 0:
                chan_x(i, c, True).wait_send()
        for h in range(2):
            upd_core(i, h, True).wait_send()
            if i > 0:
                upd_x(i, h, True).wait_send()
    upd_z().wait_send()
    for s in range(n):

        @pl.when(core_of(s) != core)
        def _():
            sum1(s).wait_send()

        @pl.when((core_of(s) == core) & (x_of(s) != x))
        def _():
            sum2(s).wait_send()

    for j in range(per):
        sum3(j).wait_send()


def per_device(
    n,
    ntp,
    resid,
    mixer_in,
    log_step,
    decay_real,
    frequency,
    input_matrix,
    output_matrix,
    skip_gain,
    value_weight,
    gate_weight,
    norm_gain,
    up_weight,
    down_weight,
):
    tokens, width = mixer_in.shape
    groups, states = decay_real.shape
    each = width // groups
    bunch = min(128 // each, groups)
    chunks = groups // bunch
    lanes = bunch * states
    features, units = value_weight.shape[0], up_weight.shape[1] // 2
    block = up_weight.shape[0]
    length = tokens // segments
    row = np.arange(tokens)
    perm = (row[None, :] == ((row % segments) * length + row // segments)[:, None]).astype(np.float32)
    nz, nx, per, pieces = n // 2, ntp // 2, n // ntp, 2
    total = groups * states
    dma = pltpu.SemaphoreType.DMA
    vmem = pl.BlockSpec(memory_space=pltpu.VMEM)
    hbm = pl.BlockSpec(memory_space=pl.ANY)
    return pl.pallas_call(
        functools.partial(kernel, n, ntp),
        out_shape=jax.ShapeDtypeStruct((tokens, width), bf16),
        in_specs=[vmem] * 8 + [hbm] * 2 + [vmem] + [hbm] * 2 + [vmem] * 2,
        out_specs=vmem,
        scratch_shapes=[
            pltpu.VMEM((features, units), bf16),
            pltpu.VMEM((features, units), bf16),
            pltpu.VMEM((features, width), bf16),
            pltpu.VMEM((features, width), bf16),
            pltpu.VMEM((tokens, total), f32),
            pltpu.VMEM((tokens, total), f32),
            pltpu.VMEM((tokens, total), f32),
            pltpu.VMEM((tokens, total), f32),
            pltpu.VMEM((tokens, lanes), f32),
            pltpu.VMEM((tokens, 2 * lanes), f32),
            pltpu.VMEM((4, segments, total), f32),
            pltpu.VMEM((n, 4, total), f32),
            pltpu.VMEM((2, segments, total), f32),
            pltpu.VMEM((tokens, width), bf16),
            pltpu.VMEM((ntp, tokens, width), bf16),
            pltpu.VMEM((2, ntp, tokens, width), bf16),
            pltpu.VMEM((tokens, features), bf16),
            pltpu.VMEM((2 * tokens, units), bf16),
            pltpu.VMEM((n, 2 * tokens, block), f32),
            pltpu.VMEM((n, 2 * tokens, block), bf16),
            pltpu.VMEM((n, 2 * tokens, block), bf16),
            pltpu.VMEM((n, 2 * tokens, block), bf16),
            pltpu.VMEM((per, nx, 2 * tokens, block), bf16),
            pltpu.VMEM((per, tokens, block), bf16),
            pltpu.VMEM((per, tokens, block), bf16),
            dma((4,)),
            dma((2, nz, pieces)),
            dma((2, nz, pieces)),
            dma((2, nz, pieces)),
            dma((2, nz, pieces)),
            dma((n - 1,)),
            dma((n - 1,)),
            dma((nx, chunks)),
            dma((nx, chunks)),
            dma((max(nx - 1, 1), chunks)),
            dma((max(nx - 1, 1), chunks)),
            dma((1,)),
            dma((1,)),
            dma((nx, 2)),
            dma((nx, 2)),
            dma((max(nx - 1, 1), 2)),
            dma((max(nx - 1, 1), 2)),
            dma((n,)),
            dma((n,)),
            dma((n,)),
            dma((per, nx)),
            dma((per,)),
            dma((per,)),
        ],
        compiler_params=pltpu.CompilerParams(
            collective_id=0, has_side_effects=True, vmem_limit_bytes=64 * 1024 * 1024 - 65536
        ),
    )(
        resid,
        mixer_in,
        log_step.T,
        decay_real,
        frequency,
        jnp.transpose(input_matrix, (0, 1, 3, 2)).reshape(2, width, states),
        output_matrix.reshape(2, width, states),
        skip_gain.reshape(1, width),
        value_weight,
        gate_weight,
        norm_gain.reshape(1, features),
        up_weight,
        down_weight,
        jnp.asarray(perm, bf16),
        jnp.asarray(perm.T, bf16),
    )


def solution(mesh):
    in_specs = (
        P("sp", "tp"),
        P("sp", "tp"),
        P("sp", "tp"),
        P("tp", None),
        P("tp", None),
        P(None, "tp", None, None),
        P(None, "tp", None, None),
        P("tp"),
        P(None, "tp"),
        P(None, "tp"),
        P(),
        P("sp", "tp"),
        P("sp", "tp"),
    )
    body = functools.partial(per_device, mesh.shape["sp"], mesh.shape["tp"])
    return jax.shard_map(
        body, mesh=mesh, in_specs=in_specs, out_specs=P("sp", "tp"), check_vma=False
    )
```

time: 195 us -> 159 us (0.82)
  the two profiles are of different devices: /device:TPU:0 before, /device:TPU:24 now
where the time goes in v1:
time: 159 us
  Pallas kernels  157 us (99%)
  local copies, waits for them, and re-layouts  1.77 us (1%)
    pallas_call x1, Pallas kernels, per_device(): pl.pallas_call(functools.partial(kernel, n, ntp), out_shape=jax.ShapeDtyp...  157 us

profile of v1, /device:TPU:24, one launch (start us, length us, event | category | flops | bytes accessed | tf_op | source)
XLA Modules:
  0.0 158.9 jit_solution(9232060586759531099)
XLA Ops:
  0.0 157.1 %shard_map.145 = bf16[384,512]{1,0:T(8,128)(2,1)} custom-call(bf16[384,512]{1,0:T(8,128)(2,1)} %resid_ref.1, bf16[384,512]{1,0:T(8,128)(2,1)} %mixer_ref.1, f32[32,384]{1,0:T(8,128)} %bitcast.9, f32[32,64]{1,0:T(8,128)} %decay_ref.1, f32[32,64]{1,0:T(8,128)} %angle_ref.1, f32[2,512,64]{2,1,0:T(8,128)} %bitcast.7, f32[2,512,64]{2,1,0:T(8,128)} %bitcast.8, ...), custom_call_target="tpu_custom_call" | custom-call | tf_op jit(solution)/shard_map/pallas_call | solution.py:740
  157.1 1.8 %copy.17 = bf16[384,512]{1,0:T(8,128)(2,1)} copy(bf16[384,512]{1,0:T(8,128)(2,1)} %shard_map.145) | data formatting | bytes 786432

commit v2 on v1

--- a/solution.py
+++ b/solution.py
@@ -176,12 +176,16 @@
             device_id_type=MESH,
         )
 
-    def z_start(which, k):
-        for part in range(pieces):
+    def z_start(which, ks, first=0, last=None):
+        for part, k in [(p, k) for p in range(pieces) for k in ks][first:last]:
             z_copy(which, k, xor(z, k), part, True).start()
 
-    def forward(which, k, zk):
-        for part in range(pieces):
+    beyond = range(2, nz)
+    many = pieces * len(beyond)
+    early, before, quarter = (5 * many) // 8, (6 * many) // 8, many // 4
+
+    def forward(which, k, zk, first=0, last=pieces):
+        for part in range(first, last):
             z_copy(which, k, zk, part, False).wait_recv()
             y_copy(which, k, zk, part, True).start()
 
@@ -204,21 +208,19 @@
         )
         c.start()
         own.append(c)
-    for which in range(2):
-        for part in range(pieces):
-            y_copy(which, 0, z, part, True).start()
-        z_start(which, 1)
-    for k in range(2, nz):
-        z_start(0, k)
+    for part in range(pieces):
+        y_copy(0, 0, z, part, True).start()
+    z_start(0, (1,))
+
+    @pl.when(inner == 1)
+    def _():
+        z_start(0, beyond, 0, early)
+
     gates = []
     for which, (source, target) in enumerate(((value_hbm, value_ref), (gate_hbm, gate_ref))):
         c = pltpu.make_async_copy(source, target, own_sem.at[2 + which])
         c.start()
         gates.append(c)
-
-    def far_down():
-        for k in range(2, nz):
-            z_start(1, k)
 
     def tp_at(a, b):
         return 2 * a + b
@@ -354,8 +356,6 @@
         last = lax.fori_loop(0, length, one, (zero + 1.0, zero, zero, zero), unroll=2)
         for i in range(4):
             ends[i, :, cols] = last[i]
-        if c >= chunks - 2:
-            forward(c - chunks + 2, 1, pair_z)
 
     def link(earlier, later):
         return (
@@ -397,6 +397,22 @@
         entry[0, s : s + 1, :] = cr
         entry[1, s : s + 1, :] = ci
         cr, ci = link((cr, ci), tuple(ends[i, s : s + 1, :] for i in range(4)))
+
+    @pl.when(inner == 1)
+    def _():
+        z_start(0, beyond, early)
+        z_start(1, (1,))
+
+    @pl.when(inner == 0)
+    def _():
+        z_start(0, beyond, 0, before)
+
+    forward(0, 1, pair_z)
+    half_way = pieces // 2
+    for k, zk in near:
+        forward(0, k, zk, 0, half_way)
+    for part in range(pieces):
+        y_copy(1, 0, z, part, True).start()
 
     for c in range(chunks):
         cols = pl.ds(c * lanes, lanes)
@@ -435,12 +451,6 @@
         if c >= 2:
             chan_forward(c - 2)
 
-    @pl.when(inner == 1)
-    def _():
-        far_down()
-
-    for k, zk in near + distant:
-        forward(0, k, zk)
     for c in range(max(chunks - 2, 0), chunks):
         chan_forward(c)
     for c in gates:
@@ -501,8 +511,19 @@
 
     @pl.when(inner == 0)
     def _():
-        far_down()
-
+        z_start(0, beyond, before)
+        z_start(1, beyond)
+        z_start(1, (1,))
+
+    @pl.when(inner == 1)
+    def _():
+        z_start(1, beyond, 0, quarter)
+
+    most = (3 * pieces) // 4
+    for k, zk in distant:
+        forward(0, k, zk, 0, most)
+    for k, zk in near:
+        forward(0, k, zk, half_way)
     for i in range(1, nx):
         upd_x(i, 0, False).wait_recv()
         upd_core(i, 0, True).start()
@@ -510,6 +531,12 @@
     for i in range(1, nx):
         upd_x(i, 1, True).start()
     upd_core(0, 1, True).start()
+    for k, zk in distant:
+        forward(0, k, zk, most)
+
+    @pl.when(inner == 0)
+    def _():
+        forward(1, 1, pair_z)
 
     def normalize(h):
         for i in range(nx):
@@ -521,29 +548,28 @@
         inv = lax.rsqrt(total * (1.0 / (width * ntp)) + rms_eps)
         for q in range(ntp):
             cols = slice(q * width, (q + 1) * width)
-            normed[:, cols] = (upd[h, q].astype(f32) * inv * gain_ref[0:1, cols]).astype(bf16)
-
-    def raise_up(h):
-        @pl.loop(0, units // tile)
-        def _(t):
-            cols = pl.ds(pl.multiple_of(t * tile, tile), tile)
-            r = jnp.dot(normed[...], up_whole[:, cols], preferred_element_type=f32)
-            r = jnp.maximum(r, 0.0)
-            hidden[h * tokens : (h + 1) * tokens, cols] = (r * r).astype(bf16)
+            normed[h * tokens : (h + 1) * tokens, cols] = (upd[h, q].astype(f32) * inv * gain_ref[0:1, cols]).astype(bf16)
 
     normalize(0)
+    for i in range(1, nx):
+        upd_x(i, 1, False).wait_recv()
+        upd_core(i, 1, True).start()
+    normalize(1)
     for c in own:
         c.wait()
     y_arrived(0, 0, z)
     y_arrived(0, 1, pair_z)
     for k, zk in far:
         y_arrived(0, k, zk)
-    raise_up(0)
-    for i in range(1, nx):
-        upd_x(i, 1, False).wait_recv()
-        upd_core(i, 1, True).start()
-    normalize(1)
-    raise_up(1)
+
+    @pl.loop(0, units // tile)
+    def _(t):
+        cols = pl.ds(pl.multiple_of(t * tile, tile), tile)
+        for h in range(2):
+            some = slice(h * tokens, (h + 1) * tokens)
+            r = jnp.dot(normed[some, :], up_whole[:, cols], preferred_element_type=f32)
+            r = jnp.maximum(r, 0.0)
+            hidden[some, cols] = (r * r).astype(bf16)
 
     def sum1(s):
         return pltpu.make_async_remote_copy(
@@ -558,20 +584,20 @@
     def sum2(s):
         return pltpu.make_async_remote_copy(
             src_ref=out2.at[s],
-            dst_ref=in2.at[s % per, x],
+            dst_ref=in2.at[s],
             send_sem=sum2_send.at[s],
-            recv_sem=sum2_recv.at[s % per, x],
-            device_id=(sp, s // per),
-            device_id_type=MESH,
-        )
-
-    def sum3(j):
-        return pltpu.make_async_remote_copy(
-            src_ref=out3.at[j],
-            dst_ref=in3.at[j],
-            send_sem=sum3_send.at[j],
-            recv_sem=sum3_recv.at[j],
+            recv_sem=sum2_recv.at[s],
             device_id=(pair, tp),
+            device_id_type=MESH,
+        )
+
+    def sum3(s, there, to):
+        return pltpu.make_async_remote_copy(
+            src_ref=out3.at[s],
+            dst_ref=in3.at[s % per, there],
+            send_sem=sum3_send.at[s],
+            recv_sem=sum3_recv.at[s % per, there],
+            device_id=(sp, to),
             device_id_type=MESH,
         )
 
@@ -603,73 +629,83 @@
         @pl.when(core_of(s) == core)
         def _():
             sum1(s).wait_recv()
-            total = keep[s] + in1[s].astype(f32)
+            out2[s] = (keep[s, tokens:] + in1[s, tokens:].astype(f32)).astype(bf16)
+            sum2(s).start()
+            keep[s, :tokens] = keep[s, :tokens] + in1[s, :tokens].astype(f32)
+
+    def stage3(s):
+        @pl.when(core_of(s) == core)
+        def _():
+            sum2(s).wait_recv()
+            total = keep[s, :tokens] + in2[s].astype(f32)
 
             @pl.when(x_of(s) == x)
             def _():
-                keep[s] = total
+                keep[s, :tokens] = total
 
             @pl.when(x_of(s) != x)
             def _():
-                out2[s] = total.astype(bf16)
-                sum2(s).start()
-
-    def stage3(s):
-        j = s % per
-
-        @pl.when(s // per == tp)
-        def _():
-            total = keep[s]
-            for i in range(1, nx):
-                there = (x + i) % nx
-                pltpu.make_async_remote_copy(
-                    src_ref=out2.at[s],
-                    dst_ref=in2.at[j, there],
-                    send_sem=sum2_send.at[s],
-                    recv_sem=sum2_recv.at[j, there],
-                    device_id=(sp, tp_at(there, core)),
-                    device_id_type=MESH,
-                ).wait_recv()
-                total += in2[j, there].astype(f32)
-            keep[s] = total
-            out3[j] = total[tokens:].astype(bf16)
-            sum3(j).start()
-
-    order = []
+                out3[s] = total.astype(bf16)
+                sum3(s, x, s // per).start()
 
     def step(k, zk, side):
         if side == 1:
             y_arrived(1, k, zk)
         s = 2 * zk + (y if side == 0 else 1 - y)
         stage1(s)
+        if order and settled[-1] != len(order):
+            stage2(order[-1])
         order.append(s)
-        if len(order) > 1:
-            stage2(order[-2])
-        if len(order) > 3:
-            stage3(order[-4])
-
-    for k, zk in near:
-        forward(1, k, zk)
+
+    order, settled = [], [0]
+
+    def settle(count):
+        stage2(order[-1])
+        settled.append(len(order))
+        for s in order[count:]:
+            stage3(s)
+
+    for k, zk in distant:
+        forward(1, k, zk, 0, half_way)
     for side in range(2):
         step(0, z, side)
+
+    @pl.when(inner == 1)
+    def _():
+        z_start(1, beyond, quarter)
+
+    for k, zk in distant:
+        forward(1, k, zk, half_way)
+    for k, zk in near:
+        forward(1, k, zk, 0, pieces // 4)
+    for k, zk in distant:
+        for side in range(2):
+            step(k, zk, side)
+
+    @pl.when(inner == 1)
+    def _():
+        forward(1, 1, pair_z)
+
+    for k, zk in near:
+        forward(1, k, zk, pieces // 4, half_way)
     for side in range(2):
         step(1, pair_z, side)
+    settle(0)
+    for k, zk in near:
+        forward(1, k, zk, half_way)
+    done = len(order)
     for k, zk in near:
         for side in range(2):
             step(k, zk, side)
-    for k, zk in distant:
-        forward(1, k, zk)
-    for k, zk in distant:
-        for side in range(2):
-            step(k, zk, side)
-    stage2(order[-1])
-    for s in order[-3:]:
-        stage3(s)
+    settle(done)
     for j in range(per):
         s = tp * per + j
-        sum3(j).wait_recv()
         cols = slice(j * block, (j + 1) * block)
-        total = keep[s, :tokens] + in3[j].astype(f32)
+        total = keep[s, :tokens]
+        for i in range(1, nx):
+            there = (x + i) % nx
+            sum3(s, there, tp_at(there, core)).wait_recv()
+            total += in3[j, there].astype(f32)
         out_ref[:, cols] = (upd[0, tp, :, cols].astype(f32) + total).astype(bf16)
 
     for which in range(2):
@@ -696,12 +732,13 @@
         def _():
             sum1(s).wait_send()
 
+        @pl.when(core_of(s) == core)
+        def _():
+            sum2(s).wait_send()
+
         @pl.when((core_of(s) == core) & (x_of(s) != x))
         def _():
-            sum2(s).wait_send()
-
-    for j in range(per):
-        sum3(j).wait_send()
+            sum3(s, x, s // per).wait_send()
 
 
 def per_device(
@@ -732,7 +769,7 @@
     length = tokens // segments
     row = np.arange(tokens)
     perm = (row[None, :] == ((row % segments) * length + row // segments)[:, None]).astype(np.float32)
-    nz, nx, per, pieces = n // 2, ntp // 2, n // ntp, 2
+    nz, nx, per, pieces = n // 2, ntp // 2, n // ntp, 4
     total = groups * states
     dma = pltpu.SemaphoreType.DMA
     vmem = pl.BlockSpec(memory_space=pltpu.VMEM)
@@ -759,15 +796,15 @@
             pltpu.VMEM((tokens, width), bf16),
             pltpu.VMEM((ntp, tokens, width), bf16),
             pltpu.VMEM((2, ntp, tokens, width), bf16),
-            pltpu.VMEM((tokens, features), bf16),
+            pltpu.VMEM((2 * tokens, features), bf16),
             pltpu.VMEM((2 * tokens, units), bf16),
             pltpu.VMEM((n, 2 * tokens, block), f32),
             pltpu.VMEM((n, 2 * tokens, block), bf16),
             pltpu.VMEM((n, 2 * tokens, block), bf16),
-            pltpu.VMEM((n, 2 * tokens, block), bf16),
-            pltpu.VMEM((per, nx, 2 * tokens, block), bf16),
-            pltpu.VMEM((per, tokens, block), bf16),
-            pltpu.VMEM((per, tokens, block), bf16),
+            pltpu.VMEM((n, tokens, block), bf16),
+            pltpu.VMEM((n, tokens, block), bf16),
+            pltpu.VMEM((n, tokens, block), bf16),
+            pltpu.VMEM((per, nx, tokens, block), bf16),
             dma((4,)),
             dma((2, nz, pieces)),
             dma((2, nz, pieces)),
@@ -788,9 +825,9 @@
             dma((n,)),
             dma((n,)),
             dma((n,)),
+            dma((n,)),
+            dma((n,)),
             dma((per, nx)),
-            dma((per,)),
-            dma((per,)),
         ],
         compiler_params=pltpu.CompilerParams(
             collective_id=0, has_side_effects=True, vmem_limit_bytes=64 * 1024 * 1024 - 65536

time: 159 us -> 135 us (0.85)
  the two profiles are of different devices: /device:TPU:24 before, /device:TPU:29 now
where the time goes in v2:
time: 135 us; the launch traced here: 133 us
  Pallas kernels  131 us (97%)
  local copies, waits for them, and re-layouts  1.77 us (1%)
    pallas_call x1, Pallas kernels, per_device(): pl.pallas_call(functools.partial(kernel, n, ntp), out_shape=jax.ShapeDtyp...  131 us

profile of v2, /device:TPU:29, one launch (start us, length us, event | category | flops | bytes accessed | tf_op | source)
XLA Modules:
  0.0 133.2 jit_solution(159701922683214628)
XLA Ops:
  0.0 131.4 %shard_map.145 = bf16[384,512]{1,0:T(8,128)(2,1)} custom-call(bf16[384,512]{1,0:T(8,128)(2,1)} %resid_ref.1, bf16[384,512]{1,0:T(8,128)(2,1)} %mixer_ref.1, f32[32,384]{1,0:T(8,128)} %bitcast.9, f32[32,64]{1,0:T(8,128)} %decay_ref.1, f32[32,64]{1,0:T(8,128)} %angle_ref.1, f32[2,512,64]{2,1,0:T(8,128)} %bitcast.7, f32[2,512,64]{2,1,0:T(8,128)} %bitcast.8, ...), custom_call_target="tpu_custom_call" | custom-call | tf_op jit(solution)/shard_map/pallas_call | solution.py:777
  131.5 1.8 %copy.17 = bf16[384,512]{1,0:T(8,128)(2,1)} copy(bf16[384,512]{1,0:T(8,128)(2,1)} %shard_map.145) | data formatting | bytes 786432

commit v3 on v2

--- a/solution.py
+++ b/solution.py
@@ -62,6 +62,8 @@
     proj,
     ends,
     carries,
+    mate,
+    prefix,
     entry,
     mixer_perm,
     chan,
@@ -110,7 +112,7 @@
     chunks = groups // bunch
     lanes, kin = bunch * states, bunch * each
     length = tokens // segments
-    pieces = z_send.shape[2]
+    pieces = z_recv.shape[2]
     piece = block // pieces
     nz, nx, per = n // 2, ntp // 2, n // ntp
     z, y = sp // 2, sp % 2
@@ -155,7 +157,7 @@
         return pltpu.make_async_remote_copy(
             src_ref=sources[which].at[pl.ds(part * piece, piece), columns_for(zk)],
             dst_ref=wholes[which].at[rows_of(owner, part)],
-            send_sem=z_send.at[which, k, part],
+            send_sem=z_send.at[which, k],
             recv_sem=z_recv.at[which, k, part],
             device_id=(2 * zk + y, tp),
             device_id_type=MESH,
@@ -170,7 +172,7 @@
         return pltpu.make_async_remote_copy(
             src_ref=src,
             dst_ref=slot,
-            send_sem=y_send.at[which, k, part],
+            send_sem=y_send.at[which, k],
             recv_sem=y_recv.at[which, k, part],
             device_id=(2 * z + 1 - y, tp),
             device_id_type=MESH,
@@ -363,56 +365,106 @@
             later[0] * earlier[1] + later[1] * earlier[0] + later[3],
         )
 
-    pr, pi, sr, si = (ends[i, 0:1, :] for i in range(4))
+    def chain(first, second):
+        fr, fi, ur, ui = first
+        qr, qi, tr, ti = second
+        vr, vi = link((ur, ui), second)
+        return qr * fr - qi * fi, qr * fi + qi * fr, vr, vi
+
+    def four(ref, *at):
+        return tuple(ref[(*at, slice(i, i + 1), slice(None))] for i in range(4))
+
+    whole_run = tuple(ends[i, 0:1, :] for i in range(4))
     for s in range(1, segments):
-        qr, qi, tr, ti = (ends[i, s : s + 1, :] for i in range(4))
-        pr, pi = qr * pr - qi * pi, qr * pi + qi * pr
-        sr, si = link((sr, si), (qr, qi, tr, ti))
-    for i, v in enumerate((pr, pi, sr, si)):
-        carries[sp, i : i + 1, :] = v
+        whole_run = chain(whole_run, tuple(ends[i, s : s + 1, :] for i in range(4)))
+    for i, v in enumerate(whole_run):
+        mate[y, i : i + 1, :] = v
+
+    def mate_copy(sending):
+        slot = y if sending else 1 - y
+        return pltpu.make_async_remote_copy(
+            src_ref=mate.at[slot],
+            dst_ref=mate.at[slot],
+            send_sem=carry_send.at[0],
+            recv_sem=carry_recv.at[0],
+            device_id=(2 * z + 1 - y, tp),
+            device_id_type=MESH,
+        )
 
     def carry_copy(i, sending):
-        there = (sp + i) % n
-        slot = sp if sending else (sp + n - i) % n
+        slot = z if sending else (z + nz - i) % nz
         return pltpu.make_async_remote_copy(
             src_ref=carries.at[slot],
             dst_ref=carries.at[slot],
-            send_sem=carry_send.at[i - 1],
-            recv_sem=carry_recv.at[i - 1],
-            device_id=(there, tp),
-            device_id_type=MESH,
-        )
-
-    for i in range(1, n):
-        carry_copy(i, True).start()
-    for i in range(1, n):
-        carry_copy(i, False).wait_recv()
-    cr = jnp.zeros_like(pr)
-    ci = jnp.zeros_like(pr)
-    for d in range(n - 1):
-        nr, ni = link((cr, ci), tuple(carries[d, i : i + 1, :] for i in range(4)))
-        cr = jnp.where(d < sp, nr, cr)
-        ci = jnp.where(d < sp, ni, ci)
+            send_sem=carry_send.at[i],
+            recv_sem=carry_recv.at[i],
+            device_id=(2 * ((z + i) % nz) + y, tp),
+            device_id_type=MESH,
+        )
+
+    upper = z // (nz // 2)
+
+    def second_sends():
+        @pl.when(inner == 1)
+        def _():
+            z_start(0, beyond, early)
+
+        @pl.when(inner == 0)
+        def _():
+            z_start(0, beyond, 0, before)
+
+    pl.when(upper == 1)(second_sends)
+    mate_copy(True).start()
+    for part in range(pieces):
+        y_copy(1, 0, z, part, True).start()
+    mate_copy(False).wait_recv()
+    for i, v in enumerate(chain(four(mate, 0), four(mate, 1))):
+        carries[z, i : i + 1, :] = v
+    for i in range(1, nz):
+
+        @pl.when(z + i < nz)
+        def _():
+            carry_copy(i, True).start()
+
+    prefix[...] = jnp.zeros_like(prefix)
+
+    def extend(run):
+        for i, v in enumerate(link((prefix[0:1, :], prefix[1:2, :]), run)):
+            prefix[i : i + 1, :] = v
+
+    for i in range(1, nz):
+
+        @pl.when(z >= i)
+        def _():
+            carry_copy(i, False).wait_recv()
+
+    for i in range(1, nz):
+
+        @pl.when(z + i < nz)
+        def _():
+            carry_copy(i, True).wait_send()
+
+    pl.when(upper == 0)(second_sends)
+
+    for d in range(nz - 1):
+
+        @pl.when(d < z)
+        def _():
+            extend(four(carries, d))
+
+    @pl.when(y == 1)
+    def _():
+        extend(four(mate, 0))
+
+    cr, ci = prefix[0:1, :], prefix[1:2, :]
     for s in range(segments):
         entry[0, s : s + 1, :] = cr
         entry[1, s : s + 1, :] = ci
         cr, ci = link((cr, ci), tuple(ends[i, s : s + 1, :] for i in range(4)))
-
-    @pl.when(inner == 1)
-    def _():
-        z_start(0, beyond, early)
-        z_start(1, (1,))
-
-    @pl.when(inner == 0)
-    def _():
-        z_start(0, beyond, 0, before)
-
     forward(0, 1, pair_z)
     half_way = pieces // 2
     for k, zk in near:
         forward(0, k, zk, 0, half_way)
-    for part in range(pieces):
-        y_copy(1, 0, z, part, True).start()
 
     for c in range(chunks):
         cols = pl.ds(c * lanes, lanes)
@@ -512,12 +564,14 @@
     @pl.when(inner == 0)
     def _():
         z_start(0, beyond, before)
-        z_start(1, beyond)
+        for k in beyond:
+            z_start(1, (k,))
         z_start(1, (1,))
 
     @pl.when(inner == 1)
     def _():
         z_start(1, beyond, 0, quarter)
+        z_start(1, (1,))
 
     most = (3 * pieces) // 4
     for k, zk in distant:
@@ -534,10 +588,6 @@
     for k, zk in distant:
         forward(0, k, zk, most)
 
-    @pl.when(inner == 0)
-    def _():
-        forward(1, 1, pair_z)
-
     def normalize(h):
         for i in range(nx):
             upd_core(i, h, False).wait_recv()
@@ -555,6 +605,11 @@
         upd_x(i, 1, False).wait_recv()
         upd_core(i, 1, True).start()
     normalize(1)
+
+    @pl.when(inner == 0)
+    def _():
+        forward(1, 1, pair_z)
+
     for c in own:
         c.wait()
     y_arrived(0, 0, z)
@@ -648,22 +703,47 @@
                 out3[s] = total.astype(bf16)
                 sum3(s, x, s // per).start()
 
-    def step(k, zk, side):
+    def step(k, zk, side, eager=False):
         if side == 1:
             y_arrived(1, k, zk)
         s = 2 * zk + (y if side == 0 else 1 - y)
         stage1(s)
-        if order and settled[-1] != len(order):
-            stage2(order[-1])
+        if waiting:
+            stage2(waiting.pop())
+        if eager:
+            stage2(s)
+        else:
+            waiting.append(s)
         order.append(s)
 
-    order, settled = [], [0]
-
-    def settle(count):
-        stage2(order[-1])
-        settled.append(len(order))
-        for s in order[count:]:
-            stage3(s)
+    order, waiting = [], []
+
+    def weights_sent(which):
+        slot = wholes[which].at[rows_of(sp)]
+        for k in range(nz):
+            for sem in (y_send, z_send)[: 1 + (k > 0)]:
+                pltpu.make_async_remote_copy(
+                    src_ref=slot,
+                    dst_ref=slot,
+                    send_sem=sem.at[which, k],
+                    recv_sem=z_recv.at[which, k, 0],
+                    device_id=(2 * z + 1 - y, tp),
+                    device_id_type=MESH,
+                ).wait_send()
+
+    def first_sent():
+        weights_sent(0)
+        mate_copy(True).wait_send()
+        for i in range(nx):
+            for c in range(chunks):
+                chan_core(i, c, True).wait_send()
+                if i > 0:
+                    chan_x(i, c, True).wait_send()
+            for h in range(2):
+                upd_core(i, h, True).wait_send()
+                if i > 0:
+                    upd_x(i, h, True).wait_send()
+        upd_z().wait_send()
 
     for k, zk in distant:
         forward(1, k, zk, 0, half_way)
@@ -676,11 +756,13 @@
 
     for k, zk in distant:
         forward(1, k, zk, half_way)
+
     for k, zk in near:
         forward(1, k, zk, 0, pieces // 4)
     for k, zk in distant:
         for side in range(2):
             step(k, zk, side)
+    stage2(waiting.pop())
 
     @pl.when(inner == 1)
     def _():
@@ -688,16 +770,26 @@
 
     for k, zk in near:
         forward(1, k, zk, pieces // 4, half_way)
+    for s in order[2:]:
+        stage3(s)
     for side in range(2):
         step(1, pair_z, side)
-    settle(0)
+    stage2(waiting.pop())
+    first_sent()
     for k, zk in near:
-        forward(1, k, zk, half_way)
+        forward(1, k, zk, half_way, most)
+    for k, zk in near:
+        forward(1, k, zk, most)
+    remaining = order[:2] + order[-2:]
     done = len(order)
-    for k, zk in near:
-        for side in range(2):
-            step(k, zk, side)
-    settle(done)
+    for side in range(2):
+        for k, zk in near:
+            step(k, zk, side, True)
+        if side == 0:
+            for s in remaining:
+                stage3(s)
+    for s in order[done:]:
+        stage3(s)
     for j in range(per):
         s = tp * per + j
         cols = slice(j * block, (j + 1) * block)
@@ -708,24 +800,7 @@
             total += in3[j, there].astype(f32)
         out_ref[:, cols] = (upd[0, tp, :, cols].astype(f32) + total).astype(bf16)
 
-    for which in range(2):
-        for k in range(nz):
-            for part in range(pieces):
-                y_copy(which, k, xor(z, k), part, True).wait_send()
-                if k > 0:
-                    z_copy(which, k, xor(z, k), part, True).wait_send()
-    for i in range(1, n):
-        carry_copy(i, True).wait_send()
-    for i in range(nx):
-        for c in range(chunks):
-            chan_core(i, c, True).wait_send()
-            if i > 0:
-                chan_x(i, c, True).wait_send()
-        for h in range(2):
-            upd_core(i, h, True).wait_send()
-            if i > 0:
-                upd_x(i, h, True).wait_send()
-    upd_z().wait_send()
+    weights_sent(1)
     for s in range(n):
 
         @pl.when(core_of(s) != core)
@@ -791,7 +866,9 @@
             pltpu.VMEM((tokens, lanes), f32),
             pltpu.VMEM((tokens, 2 * lanes), f32),
             pltpu.VMEM((4, segments, total), f32),
-            pltpu.VMEM((n, 4, total), f32),
+            pltpu.VMEM((nz, 4, total), f32),
+            pltpu.VMEM((2, 4, total), f32),
+            pltpu.VMEM((2, total), f32),
             pltpu.VMEM((2, segments, total), f32),
             pltpu.VMEM((tokens, width), bf16),
             pltpu.VMEM((ntp, tokens, width), bf16),
@@ -806,12 +883,12 @@
             pltpu.VMEM((n, tokens, block), bf16),
             pltpu.VMEM((per, nx, tokens, block), bf16),
             dma((4,)),
+            dma((2, nz)),
             dma((2, nz, pieces)),
+            dma((2, nz)),
             dma((2, nz, pieces)),
-            dma((2, nz, pieces)),
-            dma((2, nz, pieces)),
-            dma((n - 1,)),
-            dma((n - 1,)),
+            dma((nz,)),
+            dma((nz,)),
             dma((nx, chunks)),
             dma((nx, chunks)),
             dma((max(nx - 1, 1), chunks)),

time: 135 us -> 127 us (0.941); the launches traced: 133 us -> 127 us
  Pallas kernels: 131 us -> 125 us
    pallas_call x1, Pallas kernels: 131 us -> 125 us  [per_device(): pl.pallas_call(functools.partial(kernel, n, ntp), out_shape=jax.ShapeDtyp...]
where the time goes in v3:
time: 127 us
  Pallas kernels  125 us (98%)
  local copies, waits for them, and re-layouts  1.77 us (1%)
    pallas_call x1, Pallas kernels, per_device(): pl.pallas_call(functools.partial(kernel, n, ntp), out_shape=jax.ShapeDtyp...  125 us

profile of v3, /device:TPU:29, one launch (start us, length us, event | category | flops | bytes accessed | tf_op | source)
XLA Modules:
  0.0 126.8 jit_solution(2800523980025673)
XLA Ops:
  0.0 125.0 %shard_map.145 = bf16[384,512]{1,0:T(8,128)(2,1)} custom-call(bf16[384,512]{1,0:T(8,128)(2,1)} %resid_ref.1, bf16[384,512]{1,0:T(8,128)(2,1)} %mixer_ref.1, f32[32,384]{1,0:T(8,128)} %bitcast.9, f32[32,64]{1,0:T(8,128)} %decay_ref.1, f32[32,64]{1,0:T(8,128)} %angle_ref.1, f32[2,512,64]{2,1,0:T(8,128)} %bitcast.7, f32[2,512,64]{2,1,0:T(8,128)} %bitcast.8, ...), custom_call_target="tpu_custom_call" | custom-call | tf_op jit(solution)/shard_map/pallas_call | solution.py:852
  125.0 1.8 %copy.17 = bf16[384,512]{1,0:T(8,128)(2,1)} copy(bf16[384,512]{1,0:T(8,128)(2,1)} %shard_map.145) | data formatting | bytes 786432

commit v4 on v3

--- a/solution.py
+++ b/solution.py
@@ -213,6 +213,11 @@
     for part in range(pieces):
         y_copy(0, 0, z, part, True).start()
     z_start(0, (1,))
+    ahead = pieces // 2
+
+    @pl.when(inner == 0)
+    def _():
+        z_start(1, (1,), 0, ahead)
 
     @pl.when(inner == 1)
     def _():
@@ -566,12 +571,12 @@
         z_start(0, beyond, before)
         for k in beyond:
             z_start(1, (k,))
-        z_start(1, (1,))
+        z_start(1, (1,), ahead)
 
     @pl.when(inner == 1)
     def _():
         z_start(1, beyond, 0, quarter)
-        z_start(1, (1,))
+        z_start(1, (1,), 0)
 
     most = (3 * pieces) // 4
     for k, zk in distant:
@@ -606,6 +611,10 @@
         upd_core(i, 1, True).start()
     normalize(1)
 
+    @pl.when(inner == 1)
+    def _():
+        forward(1, 1, pair_z, 0, ahead)
+
     @pl.when(inner == 0)
     def _():
         forward(1, 1, pair_z)
@@ -626,32 +635,38 @@
             r = jnp.maximum(r, 0.0)
             hidden[some, cols] = (r * r).astype(bf16)
 
-    def sum1(s):
-        return pltpu.make_async_remote_copy(
-            src_ref=out1.at[s],
-            dst_ref=in1.at[s],
-            send_sem=sum1_send.at[s],
-            recv_sem=sum1_recv.at[s],
+    cuts = sum1_send.shape[1]
+    cut = block // cuts
+
+    def strip(h):
+        return slice(h * cut, (h + 1) * cut)
+
+    def sum1(s, h):
+        return pltpu.make_async_remote_copy(
+            src_ref=out1.at[s, :, pl.ds(h * cut, cut)],
+            dst_ref=in1.at[s, :, pl.ds(h * cut, cut)],
+            send_sem=sum1_send.at[s, h],
+            recv_sem=sum1_recv.at[s, h],
             device_id=(sp, partner),
             device_id_type=MESH,
         )
 
-    def sum2(s):
-        return pltpu.make_async_remote_copy(
-            src_ref=out2.at[s],
-            dst_ref=in2.at[s],
-            send_sem=sum2_send.at[s],
-            recv_sem=sum2_recv.at[s],
+    def sum2(s, h):
+        return pltpu.make_async_remote_copy(
+            src_ref=out2.at[s, :, pl.ds(h * cut, cut)],
+            dst_ref=in2.at[s, :, pl.ds(h * cut, cut)],
+            send_sem=sum2_send.at[s, h],
+            recv_sem=sum2_recv.at[s, h],
             device_id=(pair, tp),
             device_id_type=MESH,
         )
 
-    def sum3(s, there, to):
-        return pltpu.make_async_remote_copy(
-            src_ref=out3.at[s],
-            dst_ref=in3.at[s % per, there],
-            send_sem=sum3_send.at[s],
-            recv_sem=sum3_recv.at[s % per, there],
+    def sum3(s, h, there, to):
+        return pltpu.make_async_remote_copy(
+            src_ref=out3.at[s, :, pl.ds(h * cut, cut)],
+            dst_ref=in3.at[s % per, there, :, pl.ds(h * cut, cut)],
+            send_sem=sum3_send.at[s, h],
+            recv_sem=sum3_recv.at[s % per, there, h],
             device_id=(sp, to),
             device_id_type=MESH,
         )
@@ -662,13 +677,13 @@
     def x_of(s):
         return s // per // 2
 
-    def stage1(s):
-        rows = rows_of(s)
+    def stage1(s, first=0, last=cuts):
+        rows = pl.ds(pl.multiple_of(s * block + first * cut, cut), (last - first) * cut)
 
         @pl.loop(0, 2)
-        def _(h):
-            some = pl.ds(pl.multiple_of(h * tokens, tokens), tokens)
-            keep[s, some, :] = lax.dot_general(
+        def _(half):
+            some = pl.ds(pl.multiple_of(half * tokens, tokens), tokens)
+            keep[s, some, first * cut : last * cut] = lax.dot_general(
                 hidden[some, :],
                 down_whole[rows, :],
                 (((1,), (1,)), ((), ())),
@@ -677,31 +692,36 @@
 
         @pl.when(core_of(s) != core)
         def _():
-            out1[s] = keep[s].astype(bf16)
-            sum1(s).start()
-
-    def stage2(s):
+            for h in range(first, last):
+                out1[s, :, strip(h)] = keep[s, :, strip(h)].astype(bf16)
+                sum1(s, h).start()
+
+    def stage2(s, first=0, last=cuts):
         @pl.when(core_of(s) == core)
         def _():
-            sum1(s).wait_recv()
-            out2[s] = (keep[s, tokens:] + in1[s, tokens:].astype(f32)).astype(bf16)
-            sum2(s).start()
-            keep[s, :tokens] = keep[s, :tokens] + in1[s, :tokens].astype(f32)
-
-    def stage3(s):
+            for h in range(first, last):
+                w = strip(h)
+                sum1(s, h).wait_recv()
+                out2[s, :, w] = (keep[s, tokens:, w] + in1[s, tokens:, w].astype(f32)).astype(bf16)
+                sum2(s, h).start()
+                keep[s, :tokens, w] = keep[s, :tokens, w] + in1[s, :tokens, w].astype(f32)
+
+    def stage3(s, first=0, last=cuts):
         @pl.when(core_of(s) == core)
         def _():
-            sum2(s).wait_recv()
-            total = keep[s, :tokens] + in2[s].astype(f32)
-
-            @pl.when(x_of(s) == x)
-            def _():
-                keep[s, :tokens] = total
-
-            @pl.when(x_of(s) != x)
-            def _():
-                out3[s] = total.astype(bf16)
-                sum3(s, x, s // per).start()
+            for h in range(first, last):
+                w = strip(h)
+                sum2(s, h).wait_recv()
+                total = keep[s, :tokens, w] + in2[s, :, w].astype(f32)
+
+                @pl.when(x_of(s) == x)
+                def _():
+                    keep[s, :tokens, w] = total
+
+                @pl.when(x_of(s) != x)
+                def _():
+                    out3[s, :, w] = total.astype(bf16)
+                    sum3(s, h, x, s // per).start()
 
     def step(k, zk, side, eager=False):
         if side == 1:
@@ -766,54 +786,71 @@
 
     @pl.when(inner == 1)
     def _():
-        forward(1, 1, pair_z)
+        forward(1, 1, pair_z, ahead)
 
     for k, zk in near:
         forward(1, k, zk, pieces // 4, half_way)
-    for s in order[2:]:
-        stage3(s)
-    for side in range(2):
-        step(1, pair_z, side)
-    stage2(waiting.pop())
-    first_sent()
+    step(1, pair_z, 0, True)
     for k, zk in near:
         forward(1, k, zk, half_way, most)
+    for s in order[2:-1]:
+        stage3(s)
+    step(1, pair_z, 1, True)
+    first_sent()
     for k, zk in near:
         forward(1, k, zk, most)
     remaining = order[:2] + order[-2:]
-    done = len(order)
-    for side in range(2):
+    ending = []
+    for k, zk in near:
+        step(k, zk, 0, True)
+        ending.append(2 * zk + y)
+    for s in remaining:
+        stage3(s)
+    for h in range(cuts):
         for k, zk in near:
-            step(k, zk, side, True)
-        if side == 0:
-            for s in remaining:
-                stage3(s)
-    for s in order[done:]:
-        stage3(s)
+            for part in range(h * pieces // cuts, (h + 1) * pieces // cuts):
+                y_copy(1, k, zk, part, False).wait_recv()
+            s = 2 * zk + 1 - y
+            stage1(s, h, h + 1)
+            stage2(s, h, h + 1)
+        if h == 0:
+            for e in ending:
+                stage3(e)
+    weights_sent(1)
+    for s in range(n):
+
+        @pl.when(core_of(s) != core)
+        def _():
+            for h in range(cuts):
+                sum1(s, h).wait_send()
+
+    for h in range(cuts):
+        for _, zk in near:
+            stage3(2 * zk + 1 - y, h, h + 1)
+    for s in range(n):
+
+        @pl.when(core_of(s) == core)
+        def _():
+            for h in range(cuts):
+                sum2(s, h).wait_send()
+
     for j in range(per):
         s = tp * per + j
         cols = slice(j * block, (j + 1) * block)
         total = keep[s, :tokens]
         for i in range(1, nx):
             there = (x + i) % nx
-            sum3(s, there, tp_at(there, core)).wait_recv()
+            for h in range(cuts):
+                sum3(s, h, there, tp_at(there, core)).wait_recv()
             total += in3[j, there].astype(f32)
         out_ref[:, cols] = (upd[0, tp, :, cols].astype(f32) + total).astype(bf16)
 
-    weights_sent(1)
     for s in range(n):
 
-        @pl.when(core_of(s) != core)
-        def _():
-            sum1(s).wait_send()
-
-        @pl.when(core_of(s) == core)
-        def _():
-            sum2(s).wait_send()
-
         @pl.when((core_of(s) == core) & (x_of(s) != x))
         def _():
-            sum3(s, x, s // per).wait_send()
+            for h in range(cuts):
+                sum3(s, h, x, s // per).wait_send()
 
 
 def per_device(
@@ -846,6 +883,7 @@
     perm = (row[None, :] == ((row % segments) * length + row // segments)[:, None]).astype(np.float32)
     nz, nx, per, pieces = n // 2, ntp // 2, n // ntp, 4
     total = groups * states
+    cuts = 2 if block % 256 == 0 else 1
     dma = pltpu.SemaphoreType.DMA
     vmem = pl.BlockSpec(memory_space=pltpu.VMEM)
     hbm = pl.BlockSpec(memory_space=pl.ANY)
@@ -899,12 +937,12 @@
             dma((nx, 2)),
             dma((max(nx - 1, 1), 2)),
             dma((max(nx - 1, 1), 2)),
-            dma((n,)),
-            dma((n,)),
-            dma((n,)),
-            dma((n,)),
-            dma((n,)),
-            dma((per, nx)),
+            dma((n, cuts)),
+            dma((n, cuts)),
+            dma((n, cuts)),
+            dma((n, cuts)),
+            dma((n, cuts)),
+            dma((per, nx, cuts)),
         ],
         compiler_params=pltpu.CompilerParams(
             collective_id=0, has_side_effects=True, vmem_limit_bytes=64 * 1024 * 1024 - 65536

time: 127 us -> 124 us (0.976)
  Pallas kernels: 125 us -> 122 us
    pallas_call x1, Pallas kernels: 125 us -> 122 us  [per_device(): pl.pallas_call(functools.partial(kernel, n, ntp), out_shape=jax.ShapeDtyp...]
where the time goes in v4:
time: 124 us
  Pallas kernels  122 us (98%)
  local copies, waits for them, and re-layouts  1.77 us (1%)
    pallas_call x1, Pallas kernels, per_device(): pl.pallas_call(functools.partial(kernel, n, ntp), out_shape=jax.ShapeDtyp...  122 us

profile of v4, /device:TPU:29, one launch (start us, length us, event | category | flops | bytes accessed | tf_op | source)
XLA Modules:
  0.0 123.6 jit_solution(15157708465958347083)
XLA Ops:
  0.0 121.8 %shard_map.145 = bf16[384,512]{1,0:T(8,128)(2,1)} custom-call(bf16[384,512]{1,0:T(8,128)(2,1)} %resid_ref.1, bf16[384,512]{1,0:T(8,128)(2,1)} %mixer_ref.1, f32[32,384]{1,0:T(8,128)} %bitcast.9, f32[32,64]{1,0:T(8,128)} %decay_ref.1, f32[32,64]{1,0:T(8,128)} %angle_ref.1, f32[2,512,64]{2,1,0:T(8,128)} %bitcast.7, f32[2,512,64]{2,1,0:T(8,128)} %bitcast.8, ...), custom_call_target="tpu_custom_call" | custom-call | tf_op jit(solution)/shard_map/pallas_call | solution.py:890
  121.8 1.8 %copy.17 = bf16[384,512]{1,0:T(8,128)(2,1)} copy(bf16[384,512]{1,0:T(8,128)(2,1)} %shard_map.145) | data formatting | bytes 786432

commit v5 on v4

--- a/solution.py
+++ b/solution.py
@@ -804,8 +804,6 @@
     for k, zk in near:
         step(k, zk, 0, True)
         ending.append(2 * zk + y)
-    for s in remaining:
-        stage3(s)
     for h in range(cuts):
         for k, zk in near:
             for part in range(h * pieces // cuts, (h + 1) * pieces // cuts):
@@ -814,7 +812,7 @@
             stage1(s, h, h + 1)
             stage2(s, h, h + 1)
         if h == 0:
-            for e in ending:
+            for e in remaining + ending:
                 stage3(e)
     weights_sent(1)
     for s in range(n):

time: 124 us -> 123 us (level)
  no operation moved by 1% of the time
where the time goes in v5:
time: 123 us
  Pallas kernels  121 us (98%)
  local copies, waits for them, and re-layouts  1.77 us (1%)
    pallas_call x1, Pallas kernels, per_device(): pl.pallas_call(functools.partial(kernel, n, ntp), out_shape=jax.ShapeDtyp...  121 us

profile of v5, /device:TPU:29, one launch (start us, length us, event | category | flops | bytes accessed | tf_op | source)
XLA Modules:
  0.0 123.0 jit_solution(10187300902615556841)
XLA Ops:
  0.0 121.2 %shard_map.145 = bf16[384,512]{1,0:T(8,128)(2,1)} custom-call(bf16[384,512]{1,0:T(8,128)(2,1)} %resid_ref.1, bf16[384,512]{1,0:T(8,128)(2,1)} %mixer_ref.1, f32[32,384]{1,0:T(8,128)} %bitcast.9, f32[32,64]{1,0:T(8,128)} %decay_ref.1, f32[32,64]{1,0:T(8,128)} %angle_ref.1, f32[2,512,64]{2,1,0:T(8,128)} %bitcast.7, f32[2,512,64]{2,1,0:T(8,128)} %bitcast.8, ...), custom_call_target="tpu_custom_call" | custom-call | tf_op jit(solution)/shard_map/pallas_call | solution.py:888
  121.2 1.8 %copy.17 = bf16[384,512]{1,0:T(8,128)(2,1)} copy(bf16[384,512]{1,0:T(8,128)(2,1)} %shard_map.145) | data formatting | bytes 786432
